TPU v7x, 32 devices: a whole 2x2x4 slice. The times are simulated.
32 devices in a mesh: grp: 2 (over y), dp: 2 (over x), kv: 4 (over z), tp: 2 (over core).
Axes of the slice: x: 2, y: 2, z: 4, core: 2. Of those that a mesh axis runs over, the one named last changes fastest.
Arguments:
- tokens: bfloat16 [48, 2048], P(('grp', 'dp'), 'kv'), parts along dimension 0, may hold values from -24 to 24
- norm_gain: bfloat16 [2048], P('kv'), may hold values from 0.099609375 to 1.8984375
- query_weight: bfloat16 [2048, 2048], P('kv', 'tp'), may hold values from -0.125 to 0.125
- key_weight: bfloat16 [2048, 128], replicated, may hold values from -0.125 to 0.125
- value_weight: bfloat16 [2048, 128], replicated, may hold values from -0.125 to 0.125
- gate_weight: bfloat16 [2048, 2], replicated, may hold values from -0.5 to 0.5
- output_weight: bfloat16 [2048, 2048], P('tp', 'kv'), may hold values from -1 to 1
- query_gain: bfloat16 [64], replicated, may hold values from 0.099609375 to 1.8984375
- key_gain: bfloat16 [64], replicated, may hold values from 0.099609375 to 1.8984375
- key_cache: bfloat16 [48, 2, 64, 4096], P(('grp', 'dp'), 'tp', None, 'kv'), parts along dimension 0, may hold values from -1220 to 1220
- value_cache: bfloat16 [48, 2, 64, 4096], P(('grp', 'dp'), 'tp', None, 'kv'), parts along dimension 0, may hold values from -6 to 6
- decay_cache: float32 [48, 2, 4096], P(('grp', 'dp'), 'tp', 'kv'), parts along dimension 0, may hold values from -585 to 0, as said below
- lengths: int32 [48], P(('grp', 'dp')), parts along dimension 0, may hold values from 2048 to 4096, as said below
Outputs:
- mixed: bfloat16 [48, 2048], P(('grp', 'dp'), 'kv'), parts along dimension 0
- new_key: bfloat16 [48, 2, 64], P(('grp', 'dp'), 'tp'), parts along dimension 0
- new_value: bfloat16 [48, 2, 64], P(('grp', 'dp'), 'tp'), parts along dimension 0
- new_gate: float32 [48, 2], P(('grp', 'dp'), 'tp'), parts along dimension 0
There are 2 independent parts, one for each index of `grp`. A program takes and returns all parts, laid end to end along the dimension named above; an argument that names none is the same for every part. Nothing has to cross between parts.
Inputs may be any that keep to these rules, and one draw needn't show every extreme that they name: `decay_cache`: never positive, not falling as the position grows within a sequence, and zero at positions lengths - 1 and beyond. `lengths`: A sequence's cache holds positions 0 to its length - 1.
All inputs are finite; a program needn't handle non-finite values.
Results may differ from a plain program's by a relative error of at most 0.015.
The roundings to bfloat16 on the way count: a program that leaves them out, or rounds other values in their place, can miss the bound.
Values may be sent and summed in bfloat16 or wider, within the bound.
A program may use at most 64 MiB of HBM per device.

v0:
```python
import jax
import jax.numpy as jnp
from jax import lax
from jax.sharding import PartitionSpec as P

D = 2048


EPSILON = 1e-06
FLOOR = -1e30


def head_norm(values, head_gain):
    factor = lax.rsqrt(jnp.mean(values * values, axis=-1, keepdims=True) + EPSILON)
    return (values * factor * head_gain.astype(jnp.float32)).astype(jnp.bfloat16)


def on_device(
    tokens,
    norm_gain,
    query_weight,
    key_weight,
    value_weight,
    gate_weight,
    output_weight,
    query_gain,
    key_gain,
    key_cache,
    value_cache,
    decay_cache,
    lengths,
):
    head_dim = query_gain.shape[0]
    seq_count, width_here = tokens.shape
    kv_here = key_cache.shape[1]
    heads_here = query_weight.shape[1] // head_dim
    group_size = heads_here // kv_here
    span_here = key_cache.shape[3]
    kv_place = lax.axis_index("kv")
    tp_place = lax.axis_index("tp")
    row_start = kv_place * width_here
    col_start = tp_place * kv_here * head_dim
    gate_start = tp_place * kv_here
    tokens_wide = tokens.astype(jnp.float32)
    scaled = (tokens_wide * norm_gain.astype(jnp.float32)).astype(jnp.bfloat16)
    squares = jnp.sum(tokens_wide * tokens_wide, axis=1)
    key_rows = lax.dynamic_slice(
        key_weight, (row_start, col_start), (width_here, kv_here * head_dim)
    )
    value_rows = lax.dynamic_slice(
        value_weight, (row_start, col_start), (width_here, kv_here * head_dim)
    )
    gate_rows = lax.dynamic_slice(gate_weight, (row_start, gate_start), (width_here, kv_here))
    key_part = jnp.dot(scaled, key_rows, preferred_element_type=jnp.float32)
    value_part = jnp.dot(scaled, value_rows, preferred_element_type=jnp.float32)
    gate_part = jnp.dot(scaled, gate_rows, preferred_element_type=jnp.float32)
    query_table = query_weight.reshape(width_here, heads_here, head_dim)
    query_sum, key_sum, value_sum, gate_sum, square_sum = lax.psum(
        (
            jnp.einsum("sd,dhe->hse", scaled, query_table, preferred_element_type=jnp.float32),
            key_part,
            value_part,
            gate_part,
            squares,
        ),
        "kv",
    )
    queries = head_norm(query_sum, query_gain)
    row_scale = lax.rsqrt(square_sum / D + EPSILON)
    new_key = head_norm(key_sum.reshape(seq_count, kv_here, head_dim), key_gain)
    new_value = (
        (row_scale[:, None] * value_sum).astype(jnp.bfloat16).reshape(seq_count, kv_here, head_dim)
    )
    new_gate = jax.nn.log_sigmoid(row_scale[:, None] * gate_sum)
    grouped = queries.reshape(kv_here, group_size, seq_count, head_dim)
    scores = jnp.einsum(
        "kgse,skep->skgp", grouped, key_cache, preferred_element_type=jnp.float32
    ) * head_dim ** (-0.5)
    scores = scores + decay_cache[:, :, None, :] + new_gate[:, :, None, None]
    cache_positions = kv_place * span_here + lax.iota(jnp.int32, span_here)
    valid = (cache_positions[None, :] < lengths[:, None])[:, None, None, :]
    masked = jnp.where(valid, scores, FLOOR)
    block_max = jnp.max(masked, axis=3)
    weights = jnp.where(valid, jnp.exp(scores - block_max[..., None]), 0.0)
    block_total = jnp.sum(weights, axis=3)
    block_values = jnp.einsum(
        "skgp,skep->skge",
        weights.astype(jnp.bfloat16),
        value_cache,
        preferred_element_type=jnp.float32,
    )
    own = jnp.einsum(
        "kgse,ske->skg", grouped, new_key, preferred_element_type=jnp.float32
    ) * head_dim ** (-0.5)
    part_max = block_max.reshape(seq_count, heads_here)
    part_total = block_total.reshape(seq_count, heads_here)
    part_values = block_values.reshape(seq_count, heads_here * head_dim)
    global_max = lax.pmax(part_max, "kv")
    shard_scale = jnp.exp(part_max - global_max)
    rescaled_values = (
        part_values.reshape(seq_count, heads_here, head_dim) * shard_scale[..., None]
    ).reshape(seq_count, heads_here * head_dim)
    summed_total, summed_values = (
        lax.psum((part_total * shard_scale).astype(jnp.bfloat16), "kv").astype(jnp.float32),
        lax.psum(rescaled_values.astype(jnp.bfloat16), "kv").astype(jnp.float32),
    )
    merged = (global_max, summed_total, summed_values)
    all_max, all_total, all_values = merged
    own_flat = own.reshape(seq_count, heads_here)
    highest = jnp.maximum(all_max, own_flat)
    far_scale = jnp.exp(all_max - highest)
    own_scale = jnp.exp(own_flat - highest)
    total = all_total * far_scale + own_scale
    own_values = jnp.broadcast_to(
        new_value.astype(jnp.float32)[:, :, None, :], (seq_count, kv_here, group_size, head_dim)
    ).reshape(seq_count, heads_here, head_dim)
    summed = (
        all_values.reshape(seq_count, heads_here, head_dim) * far_scale[..., None]
        + own_scale[..., None] * own_values
    )
    attended = (
        (summed / total[..., None]).astype(jnp.bfloat16).reshape(seq_count, heads_here * head_dim)
    )
    partial_value = jnp.dot(attended, output_weight, preferred_element_type=jnp.float32)
    mixed = lax.psum(partial_value.astype(jnp.bfloat16), "tp")
    return (mixed, new_key, new_value, new_gate)


def solution(mesh):
    in_specs = (
        P(("grp", "dp"), "kv"),
        P("kv"),
        P("kv", "tp"),
        P(),
        P(),
        P(),
        P("tp", "kv"),
        P(),
        P(),
        P(("grp", "dp"), "tp", None, "kv"),
        P(("grp", "dp"), "tp", None, "kv"),
        P(("grp", "dp"), "tp", "kv"),
        P(("grp", "dp")),
    )
    out_specs = (
        P(("grp", "dp"), "kv"),
        P(("grp", "dp"), "tp", None),
        P(("grp", "dp"), "tp", None),
        P(("grp", "dp"), "tp"),
    )
    return jax.shard_map(
        on_device, mesh=mesh, in_specs=in_specs, out_specs=out_specs, check_vma=False
    )
```

profile of v0, /device:TPU:0, one launch (start us, length us, event | category | flops | bytes accessed | tf_op | source)
XLA Modules:
  0.0 66.7 jit_solution(15949936370953363210)
XLA Ops:
  0.6 0.0 copy-start
  0.6 0.0 copy-start.2
  0.7 0.8 %convert_element_type.58 = f32[512]{0:T(512)S(1)} convert(bf16[512]{0:T(512)(128)(2,1)} %param.14) | non-fusion elementwise | flops 512 | bytes 3072 | tf_op jit(solution)/shard_map/convert_element_type | solution.py:45
  1.5 1.1 %fusion.25 = f32[12,64]{1,0:T(8,128)S(1)} fusion(bf16[2048,128]{1,0:T(8,128)(2,1)} %param.17, s32[]{:T(128)S(6)} %select_n.26, s32[]{:T(128)S(6)} %select_n.31, bf16[12,512]{1,0:T(8,128)(2,1)} %param.13, f32[512]{0:T(512)S(1)} %convert_element_type.58), kind=kOutput, calls=%fused_computation.19 | convolution fusion | flops 804864 | bytes 152584 | tf_op jit(solution)/shard_map/dot_general | solution.py:55
  2.6 1.2 %fusion.27 = f32[12,64]{1,0:T(8,128)S(1)} fusion(bf16[2048,128]{1,0:T(8,128)(2,1)} %param.16, s32[]{:T(128)S(6)} %select_n.26, s32[]{:T(128)S(6)} %select_n.31, bf16[12,512]{1,0:T(8,128)(2,1)} %param.13, f32[512]{0:T(512)S(1)} %convert_element_type.58), kind=kOutput, calls=%fused_computation.21 | convolution fusion | flops 804864 | bytes 152584 | tf_op jit(solution)/shard_map/dot_general | solution.py:54
  3.8 0.9 %convolution_bitcast_fusion.1 = f32[12,1]{0,1:T(1,128)S(1)} fusion(bf16[12,512]{1,0:T(8,128)(2,1)} %param.13, f32[512]{0:T(512)S(1)} %convert_element_type.58, bf16[2048,2]{0,1:T(2,128)(2,1)} %param.18, s32[]{:T(128)S(6)} %select_n.26, s32[]{:T(128)S(6)} %select_n.27), kind=kOutput, calls=%fused_computation.11 | convolution fusion | flops 30720 | bytes 20536 | tf_op jit(solution)/shard_map/dot_general | solution.py:56
  4.7 0.0 copy-start.6
  4.7 0.0 copy-start.7
  4.7 0.0 copy-start.4
  4.7 0.0 copy-start.3
  4.7 1.5 %copy.19 = bf16[512,1024]{0,1:T(8,128)(2,1)S(1)} copy(bf16[512,1024]{1,0:T(8,128)(2,1)} %param.15) | data formatting | bytes 2097152 | tf_op args[2]
  6.2 0.0 copy-done.2
  6.3 0.5 convolution_bitcast_fusion
  6.8 0.1 fusion.33
  6.9 23.4 %all-reduce = (f32[12,1]{0,1:T(1,128)S(1)}, f32[12]{0:T(128)S(1)}, f32[16,12,64]{2,1,0:T(8,128)S(1)}, f32[12,64]{1,0:T(8,128)S(1)}, f32[12,64]{1,0:T(8,128)S(1)}) all-reduce(f32[12,1]{0,1:T(1,128)S(1)} %convolution_bitcast_fusion.1, f32[12]{0:T(128)S(1)} %fusion.33, ...), channel_id=1, replica_groups=mesh['grp'=2,'dp'=2,'kv'=4,'tp'=2] {'kv'}, use_global_device_ids=true, to_apply=%region_4.0 | all-reduce | flops 13848 | bytes 110784 | tf_op jit(solution)/shard_map/psum | solution.py:58
  30.3 0.7 fusion.46
  31.0 0.1 multiply_reduce_fusion.1
  31.1 0.0 copy-done.6
  31.2 0.7 %fusion.48 = (bf16[12,1,64]{2,0,1:T(8,128)(2,1)}, bf16[12,64,1]{1,0,2:T(8,128)(2,1)S(1)}) fusion(f32[64]{0:T(128)S(1)} %convert_element_type.66, f32[12,64]{1,0:T(8,128)S(1)} %get-tuple-element.7, f32[12]{0:T(128)S(1)} %add_rsqrt_fusion.1), kind=kLoop, calls=%fused_computation.61 | loop fusion | flops 2304 | bytes 6448 | tf_op jit(solution)/shard_map/convert_element_type | solution.py:15
  31.8 0.1 multiply_reduce_fusion
  31.9 0.0 copy-done.7
  32.0 0.1 multiply_convert_fusion
  32.1 0.1 fusion.29
  32.2 0.0 copy-start.5
  32.3 0.0 copy-done.4
  32.3 0.1 broadcast_compare_fusion
  32.4 0.0 copy-done.3
  32.4 0.0 copy-done
  32.4 0.4 select_reduce_fusion
  32.8 0.3 fusion.19
  33.1 0.0 copy-done.5
  33.1 8.5 %pmax.7 = f32[12,16]{1,0:T(8,128)S(1)} all-reduce(f32[12,16]{1,0:T(8,128)S(1)} %get-tuple-element.20), channel_id=1, replica_groups=mesh['grp'=2,'dp'=2,'kv'=4,'tp'=2] {'kv'}, use_global_device_ids=true, to_apply=%region_6.0 | all-reduce | flops 192 | bytes 1536 | tf_op jit(solution)/shard_map/pmax | solution.py:98
  41.7 0.0 copy-start.1
  41.7 2.1 %fusion.16 = bf16[12,16,64]{2,1,0:T(8,128)(2,1)S(1)} fusion(bf16[12,1,64,1024]{3,2,1,0:T(8,128)(2,1)} %param.23, f32[12,16,1024]{2,1,0:T(8,128)S(1)} %get-tuple-element.21, f32[12,16]{1,0:T(8,128)S(1)} %get-tuple-element.20, pred[12,1024]{1,0:T(8,128)(4,1)S(1)} %broadcast_compare_fusion, f32[12,16]{1,0:T(8,128)S(1)} %get-tuple-element.15), kind=kOutput, calls=%fused_computation.9 | convolution fusion | flops 25780224 | bytes 2397696 | tf_op jit(solution)/shard_map/skgp,skep->skge/dot_general | solution.py:86
  43.8 0.1 convert_element_type.64
  43.9 18.0 %all-reduce.1 = (bf16[12,16]{1,0:T(8,128)(2,1)S(1)}, bf16[12,1024]{1,0:T(8,128)(2,1)S(1)}) all-reduce(bf16[12,16]{1,0:T(8,128)(2,1)S(1)} %get-tuple-element.14, bf16[12,1024]{1,0:T(8,128)(2,1)S(1)} %convert_element_type.64), channel_id=1, replica_groups=mesh['grp'=2,'dp'=2,'kv'=4,'tp'=2] {'kv'}, use_global_device_ids=true, to_apply=%region_12.13 | all-reduce | flops 12480 | bytes 49920 | tf_op jit(solution)/shard_map/psum | solution.py:104
  62.0 0.1 broadcast_multiply_fusion
  62.0 0.1 mul.155
  62.1 0.1 div.27
  62.2 0.1 div.28
  62.3 0.1 mul.148
  62.4 0.1 mul.149
  62.5 0.0 copy-done.1
  62.5 0.2 convolution_convert_fusion
  62.8 4.0 %psum.63 = bf16[12,512]{1,0:T(8,128)(2,1)} all-reduce(bf16[12,512]{1,0:T(8,128)(2,1)S(1)} %convolution_convert_fusion), channel_id=1, replica_groups=mesh['grp'=2,'dp'=2,'kv'=4,'tp'=2] {'tp'}, use_global_device_ids=true, to_apply=%region_13.14 | all-reduce | flops 6144 | bytes 24576 | tf_op jit(solution)/shard_map/psum | solution.py:125
  (10 shorter events, 0.1 us)
Async XLA Ops:
  0.6 31.8 %copy-start = (bf16[12,1,64,1024]{3,2,1,0:T(8,128)(2,1)S(1)}, bf16[12,1,64,1024]{3,2,1,0:T(8,128)(2,1)}, u32[]{:S(2)}) copy-start(bf16[12,1,64,1024]{3,2,1,0:T(8,128)(2,1)} %param.22) | copy-start | bytes 4718596
  0.6 5.6 %copy-start.2 = (bf16[12,512]{1,0:T(8,128)(2,1)S(1)}, bf16[12,512]{1,0:T(8,128)(2,1)}, u32[]{:S(2)}) copy-start(bf16[12,512]{1,0:T(8,128)(2,1)} %param.13) | copy-start | bytes 36868
  4.7 26.5 %copy-start.6 = (bf16[64]{0:T(256)(128)(2,1)S(1)}, bf16[64]{0:T(256)(128)(2,1)}, u32[]{:S(2)}) copy-start(bf16[64]{0:T(256)(128)(2,1)} %param.21) | copy-start | bytes 388
  4.7 27.3 %copy-start.7 = (bf16[64]{0:T(256)(128)(2,1)S(1)}, bf16[64]{0:T(256)(128)(2,1)}, u32[]{:S(2)}) copy-start(bf16[64]{0:T(256)(128)(2,1)} %param.20) | copy-start | bytes 388
  4.7 27.6 %copy-start.4 = (s32[12]{0:T(128)S(1)}, s32[12]{0:T(128)}, u32[]{:S(2)}) copy-start(s32[12]{0:T(128)} %param.25) | copy-start | bytes 148
  4.7 27.7 %copy-start.3 = (f32[12,1,1024]{2,1,0:T(1,128)S(1)}, f32[12,1,1024]{2,1,0:T(1,128)}, u32[]{:S(2)}) copy-start(f32[12,1,1024]{2,1,0:T(1,128)} %param.24) | copy-start | bytes 147460
  32.2 0.9 %copy-start.5 = (f32[12,1]{0,1:T(1,128)}, f32[12,1]{0,1:T(1,128)S(1)}, u32[]{:S(2)}) copy-start(f32[12,1]{0,1:T(1,128)S(1)} %fusion.43) | copy-start | bytes 148
  41.7 20.8 %copy-start.1 = (bf16[1024,512]{1,0:T(8,128)(2,1)S(1)}, bf16[1024,512]{1,0:T(8,128)(2,1)}, u32[]{:S(2)}) copy-start(bf16[1024,512]{1,0:T(8,128)(2,1)} %param.19) | copy-start | bytes 3145732
where the time goes:
time: 67.2 us; the launch traced here: 66.7 us
  blocking collectives  53.9 us (80%)
  matrix products  6.57 us (10%)
  other arithmetic  3.12 us (5%)
  local copies, waits for them, and re-layouts  2.18 us (3%)
  between operations  0.9 us (1%)
    psum x1, blocking collectives, on_device(): lax.psum((jnp.einsum('sd,dhe->hse', scaled, query_table, preferred_elemen...  23.4 us
    psum x1, blocking collectives, on_device(): lax.psum((part_total * shard_scale).astype(jnp.bfloat16), 'kv')  18 us
    pmax x1, blocking collectives, on_device(): global_max = lax.pmax(part_max, 'kv')  8.52 us
    psum x1, blocking collectives, on_device(): mixed = lax.psum(partial_value.astype(jnp.bfloat16), 'tp')  3.96 us
    dot_general x1, matrix products, on_device(): jnp.einsum('skgp,skep->skge', weights.astype(jnp.bfloat16), value_cache,...  2.06 us
    unnamed x18, local copies, waits for them, and re-layouts  1.61 us

commit v1 on v0

v1 whole, which is shorter than its diff:
```python
import functools

import jax
import jax.numpy as jnp
from jax import lax
from jax.experimental import pallas as pl
from jax.experimental.pallas import tpu as pltpu
from jax.sharding import PartitionSpec as P

MESH = pl.DeviceIdType.MESH
EPSILON = 1e-06
FLOOR = -1e30
SEND_DTYPE = jnp.float32
F32 = jnp.float32
BF16 = jnp.bfloat16


def kernel(
    kv_n,
    tp_n,
    lengths_ref,
    tokens_ref,
    norm_gain_ref,
    query_gain_ref,
    key_gain_ref,
    gate_hbm,
    query_hbm,
    key_w_hbm,
    value_w_hbm,
    output_hbm,
    key_hbm,
    value_hbm,
    decay_hbm,
    mixed_ref,
    new_key_ref,
    new_value_ref,
    new_gate_ref,
    query_w,
    key_w,
    value_w,
    gate_w,
    output_w,
    keys,
    values,
    decay,
    query_slots,
    small_slots,
    value_slots,
    stat_slots,
    out_slots,
    query_rows,
    att_rows,
    local_sem,
    query_send,
    query_recv,
    small_send,
    small_recv,
    value_send,
    value_recv,
    stat_send,
    stat_recv,
    out_send,
    out_recv,
):
    rows, width = tokens_ref.shape
    group = query_rows.shape[0] // rows
    head_dim, span = keys.shape[1:]
    pairs = rows // 2
    me = lax.axis_index("kv")
    tp_me = lax.axis_index("tp")
    model = width * kv_n
    chunks = value_send.shape[1]
    per_chunk = pairs // chunks

    barrier = pltpu.get_barrier_semaphore()
    for d in range(1, kv_n):
        pl.semaphore_signal(
            barrier, inc=1, device_id={"kv": lax.rem(me + d, kv_n)}, device_id_type=MESH
        )
    for d in range(1, tp_n):
        pl.semaphore_signal(
            barrier, inc=1, device_id={"tp": lax.rem(tp_me + d, tp_n)}, device_id_type=MESH
        )

    row_start = pl.multiple_of(me * width, width)
    query_chunks = query_w.shape[0]
    query_cols = query_w.shape[2]
    query_copies = [
        pltpu.make_async_copy(
            query_hbm.at[:, pl.ds(c * query_cols, query_cols)], query_w.at[c], local_sem.at[c]
        )
        for c in range(query_chunks)
    ]
    base = query_chunks
    small_copies = [
        pltpu.make_async_copy(key_w_hbm.at[pl.ds(row_start, width)], key_w, local_sem.at[base]),
        pltpu.make_async_copy(
            value_w_hbm.at[pl.ds(row_start, width)], value_w, local_sem.at[base + 1]
        ),
        pltpu.make_async_copy(
            gate_hbm.at[:, pl.ds(row_start, width)], gate_w, local_sem.at[base + 2]
        ),
    ]
    key_copy = pltpu.make_async_copy(key_hbm.at[:, 0], keys, local_sem.at[base + 3])
    decay_copy = pltpu.make_async_copy(decay_hbm, decay, local_sem.at[base + 4])
    value_copy = pltpu.make_async_copy(value_hbm.at[:, 0], values, local_sem.at[base + 5])
    output_copy = pltpu.make_async_copy(output_hbm, output_w, local_sem.at[base + 6])
    for copy in (*query_copies, *small_copies, key_copy, decay_copy, value_copy, output_copy):
        copy.start()

    def sends(slots, send_sem, recv_sem, index=None):
        out = []
        for d in range(1, kv_n):
            ref = slots.at[me] if index is None else slots.at[me, index]
            out.append(
                pltpu.make_async_remote_copy(
                    src_ref=ref,
                    dst_ref=ref,
                    send_sem=send_sem.at[d] if index is None else send_sem.at[d, index_of(index)],
                    recv_sem=recv_sem.at[me] if index is None else recv_sem.at[me, index_of(index)],
                    device_id={"kv": lax.rem(me + d, kv_n)},
                    device_id_type=MESH,
                )
            )
        return out

    def index_of(index):
        return index if isinstance(index, int) else index.start // per_chunk

    def wait_recv(slots, send_sem, recv_sem, index=None):
        for d in range(1, kv_n):
            src = lax.rem(me + d, kv_n)
            ref = slots.at[src] if index is None else slots.at[src, index]
            pltpu.make_async_remote_copy(
                src_ref=ref,
                dst_ref=ref,
                send_sem=send_sem.at[d] if index is None else send_sem.at[d, index_of(index)],
                recv_sem=recv_sem.at[src] if index is None else recv_sem.at[src, index_of(index)],
                device_id={"kv": src},
                device_id_type=MESH,
            ).wait_recv()

    tokens = tokens_ref[...].astype(F32)
    scaled = (tokens * norm_gain_ref[...].astype(F32)).astype(BF16)
    for c in range(query_chunks):
        query_copies[c].wait()
        part = jnp.dot(scaled, query_w[c], preferred_element_type=F32)
        query_slots[me, :, pl.ds(c * query_cols, query_cols)] = part.astype(query_slots.dtype)
        if c == 0:
            pass
    pl.semaphore_wait(barrier, kv_n - 1 + tp_n - 1)
    query_sends = sends(query_slots, query_send, query_recv)
    for copy in query_sends:
        copy.start()

    lane_small = lax.broadcasted_iota(jnp.int32, (rows, 128), 1)
    row_small = lax.broadcasted_iota(jnp.int32, (rows, 128), 0)
    diagonal = lane_small == row_small
    low = lane_small < head_dim

    def to_row(column):
        return jnp.sum(jnp.where(diagonal, column, 0.0), axis=0, keepdims=True)

    def to_column(row):
        return jnp.sum(jnp.where(diagonal, row, 0.0), axis=1, keepdims=True)

    for copy in small_copies:
        copy.wait()
    key_part = jnp.dot(scaled, key_w[...], preferred_element_type=F32)
    value_part = jnp.dot(scaled, value_w[...], preferred_element_type=F32)
    key_turned = pltpu.roll(key_part, head_dim, 1)
    value_turned = pltpu.roll(value_part, head_dim, 1)
    first = tp_me == 0
    key_half = jnp.where(first, key_part, key_turned)
    value_half = jnp.where(first, value_turned, value_part)
    gates = gate_w[...].astype(F32)
    gate_row = jnp.where(first, gates[0:1], gates[1:2])
    gate_part = jnp.sum(scaled.astype(F32) * gate_row, axis=1, keepdims=True)
    squares = jnp.sum(tokens * tokens, axis=1, keepdims=True)
    small_slots[me, 0:rows] = jnp.where(low, key_half, value_half)
    small_slots[me, rows : rows + 1] = to_row(gate_part)
    small_slots[me, rows + 1 : rows + 2] = to_row(squares)
    small_slots[me, rows + 2 :] = jnp.zeros((small_slots.shape[1] - rows - 2, 128), F32)
    small_sends = sends(small_slots, small_send, small_recv)
    for copy in small_sends:
        copy.start()

    wait_recv(query_slots, query_send, query_recv)
    gain = query_gain_ref[...].astype(F32)
    gain2 = jnp.concatenate([gain, gain], axis=1)

    def norm_pair(x, gain_wide):
        squared = x * x
        lo = jnp.sum(jnp.where(low, squared, 0.0), axis=1, keepdims=True)
        hi = jnp.sum(jnp.where(low, 0.0, squared), axis=1, keepdims=True)
        lo = lax.rsqrt(lo / head_dim + EPSILON)
        hi = lax.rsqrt(hi / head_dim + EPSILON)
        return (x * jnp.where(low, lo, hi) * gain_wide).astype(BF16).astype(F32)

    for c in range(group // 2):
        cols = pl.ds(c * 128, 128)
        x = query_slots[0, :, cols].astype(F32)
        for p in range(1, kv_n):
            x = x + query_slots[p, :, cols].astype(F32)
        y = norm_pair(x, gain2)
        query_rows[pl.ds(2 * c, rows, stride=group), :] = y
        query_rows[pl.ds(2 * c + 1, rows, stride=group), :] = pltpu.roll(y, head_dim, 1)

    key_copy.wait()
    decay_copy.wait()
    value_copy.wait()
    scale = head_dim ** (-0.5)
    positions = me * span + lax.broadcasted_iota(jnp.int32, (group, span), 1)
    lane = lax.broadcasted_iota(jnp.int32, (group, 128), 1)
    stat_max = jnp.full((group, 128), FLOOR, F32)
    stat_sum = jnp.zeros((group, 128), F32)

    def attend(b, stat_max, stat_sum):
        q = query_rows[group * b : group * (b + 1), 0:head_dim].astype(BF16)
        scores = jnp.dot(q, keys[b], preferred_element_type=F32) * scale + decay[b]
        valid = positions < lengths_ref[b]
        block_max = jnp.max(jnp.where(valid, scores, FLOOR), axis=1, keepdims=True)
        weights = jnp.where(valid, jnp.exp(scores - block_max), 0.0)
        block_sum = jnp.sum(weights, axis=1, keepdims=True)
        result = lax.dot_general(
            weights.astype(BF16), values[b], (((1,), (1,)), ((), ())), preferred_element_type=F32
        )
        stat_max = jnp.where(lane == b, block_max, stat_max)
        stat_sum = jnp.where(lane == b + 32, block_sum, stat_sum)
        return result, stat_max, stat_sum

    value_sends = []
    for i in range(pairs):
        one, stat_max, stat_sum = attend(i, stat_max, stat_sum)
        two, stat_max, stat_sum = attend(i + pairs, stat_max, stat_sum)
        value_slots[me, i] = jnp.concatenate([one, two], axis=1).astype(BF16)
        if (i + 1) % per_chunk == 0:
            index = pl.ds(i + 1 - per_chunk, per_chunk)
            new = sends(value_slots, value_send, value_recv, index)
            for copy in new:
                copy.start()
            value_sends += new
    half = group // 2
    packed = jnp.where(lane < 32, stat_max, stat_sum)
    stat_slots[me] = jnp.where(
        lane[:half] < 64, packed[:half], pltpu.roll(packed[half:], 64, 1)
    )
    stat_sends = sends(stat_slots, stat_send, stat_recv)
    for copy in stat_sends:
        copy.start()

    wait_recv(small_slots, small_send, small_recv)
    small = small_slots[0]
    for p in range(1, kv_n):
        small = small + small_slots[p]
    row_scale_row = lax.rsqrt(small[rows + 1 : rows + 2] / model + EPSILON)
    gate_x = row_scale_row * small[rows : rows + 1]
    gate = jnp.minimum(gate_x, 0.0) - jnp.log1p(jnp.exp(-jnp.abs(gate_x)))
    new_gate_ref[...] = to_column(gate)
    key_gain = key_gain_ref[...].astype(F32)
    both = small[:rows]
    new_key = norm_pair(both, jnp.concatenate([key_gain, key_gain], axis=1))
    new_value = (both * to_column(row_scale_row)).astype(BF16).astype(F32)
    own = jnp.zeros((group, 128), F32)
    for b in range(rows):
        new_key_ref[b] = new_key[b : b + 1, 0:head_dim].astype(BF16)
        new_value_ref[b] = new_value[b : b + 1, head_dim:].astype(BF16)
        q = query_rows[group * b : group * (b + 1), :]
        dots = jnp.sum(
            jnp.where(lane < head_dim, q * new_key[b : b + 1], 0.0), axis=1, keepdims=True
        )
        own = jnp.where(lane == b, dots * scale, own)

    wait_recv(stat_slots, stat_send, stat_recv)
    maxima, totals = [], []
    for p in range(kv_n):
        packed = stat_slots[p]
        packed = jnp.concatenate([packed, pltpu.roll(packed, 64, 1)], axis=0)
        maxima.append(packed + gate)
        totals.append(pltpu.roll(packed, 96, 1))
    real = lane < rows
    top = own
    for p in range(kv_n):
        top = jnp.maximum(top, maxima[p])
    factors = [jnp.where(real, jnp.exp(maxima[p] - top), 0.0) for p in range(kv_n)]
    own_factor = jnp.exp(own - top)
    total = own_factor
    for p in range(kv_n):
        total = total + factors[p] * totals[p]
    total = jnp.where(real, total, 1.0)
    factors = [f / total for f in factors]
    own_factor = own_factor / total

    def spread(f, i):
        return jnp.where(lane < head_dim, f[:, i : i + 1], f[:, i + pairs : i + pairs + 1])

    new_value_turned = pltpu.roll(new_value, head_dim, 1)
    for c in range(chunks):
        wait_recv(value_slots, value_send, value_recv, pl.ds(c * per_chunk, per_chunk))
        for i in range(c * per_chunk, (c + 1) * per_chunk):
            fresh = jnp.where(
                lane[0:1] < head_dim,
                new_value_turned[i : i + 1],
                new_value[i + pairs : i + pairs + 1],
            )
            acc = spread(own_factor, i) * fresh
            for p in range(kv_n):
                acc = acc + spread(factors[p], i) * value_slots[p, i].astype(F32)
            query_rows[group * i : group * (i + 1), :] = acc

    for c in range(group // 2):
        x = query_rows[pl.ds(2 * c, pairs, stride=group), :]
        y = query_rows[pl.ds(2 * c + 1, pairs, stride=group), :]
        lo = lax.broadcasted_iota(jnp.int32, (pairs, 128), 1) < head_dim
        cols = slice(c * 128, (c + 1) * 128)
        att_rows[0:pairs, cols] = jnp.where(lo, x, pltpu.roll(y, head_dim, 1))
        att_rows[pairs:rows, cols] = jnp.where(lo, pltpu.roll(x, head_dim, 1), y)

    output_copy.wait()
    partial = jnp.dot(att_rows[...].astype(BF16), output_w[...], preferred_element_type=F32)
    out_slots[tp_me] = partial.astype(BF16)
    out_sends = []
    for d in range(1, tp_n):
        copy = pltpu.make_async_remote_copy(
            src_ref=out_slots.at[tp_me],
            dst_ref=out_slots.at[tp_me],
            send_sem=out_send.at[d],
            recv_sem=out_recv.at[tp_me],
            device_id={"tp": lax.rem(tp_me + d, tp_n)},
            device_id_type=MESH,
        )
        copy.start()
        out_sends.append(copy)
    for copy in (*query_sends, *small_sends, *value_sends, *stat_sends):
        copy.wait_send()
    for d in range(1, tp_n):
        src = lax.rem(tp_me + d, tp_n)
        pltpu.make_async_remote_copy(
            src_ref=out_slots.at[src],
            dst_ref=out_slots.at[src],
            send_sem=out_send.at[d],
            recv_sem=out_recv.at[src],
            device_id={"tp": src},
            device_id_type=MESH,
        ).wait_recv()
    mixed = out_slots[0].astype(F32)
    for t in range(1, tp_n):
        mixed = mixed + out_slots[t].astype(F32)
    mixed_ref[...] = mixed.astype(BF16)
    for copy in out_sends:
        copy.wait_send()


def on_device(
    kv_n,
    tp_n,
    tokens,
    norm_gain,
    query_weight,
    key_weight,
    value_weight,
    gate_weight,
    output_weight,
    query_gain,
    key_gain,
    key_cache,
    value_cache,
    decay_cache,
    lengths,
):
    rows, width = tokens.shape
    head_dim = query_gain.shape[0]
    heads = query_weight.shape[1] // head_dim
    span = key_cache.shape[3]
    out_cols = output_weight.shape[1]
    query_chunks = 2
    chunks = 3
    pairs = rows // 2
    small_rows = -(-(rows + 2) // 8) * 8
    vmem = pl.BlockSpec(memory_space=pltpu.VMEM)
    hbm = pl.BlockSpec(memory_space=pl.ANY)
    dma = pltpu.SemaphoreType.DMA
    return pl.pallas_call(
        functools.partial(kernel, kv_n, tp_n),
        out_shape=(
            jax.ShapeDtypeStruct((rows, out_cols), BF16),
            jax.ShapeDtypeStruct((rows, 1, head_dim), BF16),
            jax.ShapeDtypeStruct((rows, 1, head_dim), BF16),
            jax.ShapeDtypeStruct((rows, 1), F32),
        ),
        in_specs=[pl.BlockSpec(memory_space=pltpu.SMEM)] + [vmem] * 4 + [hbm] * 8,
        out_specs=(vmem, vmem, vmem, vmem),
        scratch_shapes=[
            pltpu.VMEM((query_chunks, width, heads * head_dim // query_chunks), BF16),
            pltpu.VMEM((width, key_weight.shape[1]), BF16),
            pltpu.VMEM((width, value_weight.shape[1]), BF16),
            pltpu.VMEM((gate_weight.shape[1], width), BF16),
            pltpu.VMEM(output_weight.shape, BF16),
            pltpu.VMEM((rows, head_dim, span), BF16),
            pltpu.VMEM((rows, head_dim, span), BF16),
            pltpu.VMEM((rows, 1, span), F32),
            pltpu.VMEM((kv_n, rows, heads * head_dim), SEND_DTYPE),
            pltpu.VMEM((kv_n, small_rows, 128), F32),
            pltpu.VMEM((kv_n, pairs, heads, 2 * head_dim), BF16),
            pltpu.VMEM((kv_n, heads // 2, 128), F32),
            pltpu.VMEM((tp_n, rows, out_cols), BF16),
            pltpu.VMEM((rows * heads, 128), F32),
            pltpu.VMEM((rows, heads * head_dim), F32),
            dma((query_chunks + 7,)),
            dma((kv_n,)),
            dma((kv_n,)),
            dma((kv_n,)),
            dma((kv_n,)),
            dma((kv_n, chunks)),
            dma((kv_n, chunks)),
            dma((kv_n,)),
            dma((kv_n,)),
            dma((tp_n,)),
            dma((tp_n,)),
        ],
        compiler_params=pltpu.CompilerParams(
            collective_id=0, has_side_effects=True, vmem_limit_bytes=48 * 1024 * 1024
        ),
        name="decode",
    )(
        lengths,
        tokens,
        norm_gain.reshape(1, width),
        query_gain.reshape(1, head_dim),
        key_gain.reshape(1, head_dim),
        gate_weight.T,
        query_weight,
        key_weight,
        value_weight,
        output_weight,
        key_cache,
        value_cache,
        decay_cache,
    )


def solution(mesh):
    batch = P(("grp", "dp"))
    in_specs = (
        P(("grp", "dp"), "kv"),
        P("kv"),
        P("kv", "tp"),
        P(),
        P(),
        P(),
        P("tp", "kv"),
        P(),
        P(),
        P(("grp", "dp"), "tp", None, "kv"),
        P(("grp", "dp"), "tp", None, "kv"),
        P(("grp", "dp"), "tp", "kv"),
        batch,
    )
    out_specs = (
        P(("grp", "dp"), "kv"),
        P(("grp", "dp"), "tp", None),
        P(("grp", "dp"), "tp", None),
        P(("grp", "dp"), "tp"),
    )
    return jax.shard_map(
        functools.partial(on_device, mesh.shape["kv"], mesh.shape["tp"]),
        mesh=mesh,
        in_specs=in_specs,
        out_specs=out_specs,
        check_vma=False,
    )
```

time: 67.2 us -> 36.2 us (0.54)
  blocking collectives: 53.9 us -> 0 us
  Pallas kernels: 0 us -> 21.8 us
  local copies, waits for them, and re-layouts: 2.18 us -> 13.2 us
  matrix products: 6.57 us -> 0 us
  other arithmetic: 3.12 us -> 0 us
    psum x3 -> x0, blocking collectives: 45.4 us -> none  [the longest x1 23.4 us: on_device(): lax.psum((jnp.einsum('sd,dhe->hse', scaled, query_table, preferred_elemen...]
    pallas_call x0 -> x1, Pallas kernels: none -> 21.8 us  [on_device(): pl.pallas_call(functools.partial(kernel, kv_n, tp_n), out_shape=(jax.Shap...]
    unnamed x18 -> x23, local copies, waits for them, and re-layouts: 1.61 us -> 10.7 us
    pmax x1 -> x0, blocking collectives: 8.52 us -> none  [on_device(): global_max = lax.pmax(part_max, 'kv')]
    dot_general x8 -> x0, matrix products: 6.57 us -> none  [the longest x1 2.06 us: on_device(): jnp.einsum('skgp,skep->skge', weights.astype(jnp.bfloat16), value_cache,...]
    pallas_call x0 -> x3, local copies, waits for them, and re-layouts: none -> 1.78 us  [on_device(): pl.pallas_call(functools.partial(kernel, kv_n, tp_n), out_shape=(jax.Shap...]
    convert_element_type x6 -> x0, other arithmetic: 1.58 us -> none  [the longest x1 0.8 us: on_device(): scaled = (tokens_wide * norm_gain.astype(jnp.float32)).astype(jnp.bfloat16)]
    reshape x0 -> x1, local copies, waits for them, and re-layouts: none -> 0.68 us  [on_device(): norm_gain.reshape(1, width)]
where the time goes in v1:
time: 36.2 us; the launch traced here: 35.7 us
  Pallas kernels  21.8 us (60%)
  local copies, waits for them, and re-layouts  13.2 us (36%)
  between operations  0.65 us (2%)
    pallas_call x1, Pallas kernels, on_device(): pl.pallas_call(functools.partial(kernel, kv_n, tp_n), out_shape=(jax.Shap...  21.8 us
    unnamed x23, local copies, waits for them, and re-layouts  10.7 us
    pallas_call x3, local copies, waits for them, and re-layouts, on_device(): pl.pallas_call(functools.partial(kernel, kv_n, tp_n), out_shape=(jax.Shap...  1.78 us

profile of v1, /device:TPU:0, one launch (start us, length us, event | category | flops | bytes accessed | tf_op | source)
XLA Modules:
  0.0 35.7 jit_solution(11483525958667068119)
XLA Ops:
  0.6 0.7 %reshape.17.norm_gain_ref = bf16[1,512]{1,0:T(2,128)(2,1)S(1)} reshape(bf16[512]{0:T(512)(128)(2,1)} %param.14) | data formatting | bytes 2048 | tf_op jit(solution)/shard_map/reshape | solution.py:428
  1.3 0.0 copy-start
  1.3 1.4 %copy-done = bf16[12,1,64,1024]{3,2,1,0:T(8,128)(2,1)S(1)} copy-done((bf16[12,1,64,1024]{3,2,1,0:T(8,128)(2,1)S(1)}, bf16[12,1,64,1024]{3,2,1,0:T(8,128)(2,1)}, u32[]{:S(2)}) %copy-start) | copy-done | bytes 1572888
  2.7 0.0 copy-start.1
  2.7 1.2 %copy-done.1 = bf16[512,1024]{1,0:T(8,128)(2,1)S(1)} copy-done((bf16[512,1024]{1,0:T(8,128)(2,1)S(1)}, bf16[512,1024]{1,0:T(8,128)(2,1)}, u32[]{:S(2)}) %copy-start.1) | copy-done | bytes 1048600
  3.9 0.0 copy-start.2
  3.9 1.2 %copy-done.2 = bf16[1024,512]{1,0:T(8,128)(2,1)S(1)} copy-done((bf16[1024,512]{1,0:T(8,128)(2,1)S(1)}, bf16[1024,512]{1,0:T(8,128)(2,1)}, u32[]{:S(2)}) %copy-start.2) | copy-done | bytes 1048600
  5.2 0.0 copy-start.3
  5.2 1.0 %copy-done.3 = bf16[2048,128]{1,0:T(8,128)(2,1)S(1)} copy-done((bf16[2048,128]{1,0:T(8,128)(2,1)S(1)}, bf16[2048,128]{1,0:T(8,128)(2,1)}, u32[]{:S(2)}) %copy-start.3) | copy-done | bytes 524312
  6.2 0.0 copy-start.4
  6.2 1.0 %copy-done.4 = bf16[2048,128]{1,0:T(8,128)(2,1)S(1)} copy-done((bf16[2048,128]{1,0:T(8,128)(2,1)S(1)}, bf16[2048,128]{1,0:T(8,128)(2,1)}, u32[]{:S(2)}) %copy-start.4) | copy-done | bytes 524312
  7.3 0.0 copy-start.5
  7.3 0.8 %copy-done.5 = f32[12,1,1024]{2,1,0:T(1,128)S(1)} copy-done((f32[12,1,1024]{2,1,0:T(1,128)S(1)}, f32[12,1,1024]{2,1,0:T(1,128)}, u32[]{:S(2)}) %copy-start.5) | copy-done | bytes 49176
  8.1 0.0 copy-start.6
  8.1 0.7 %copy-done.6 = bf16[12,512]{1,0:T(8,128)(2,1)S(1)} copy-done((bf16[12,512]{1,0:T(8,128)(2,1)S(1)}, bf16[12,512]{1,0:T(8,128)(2,1)}, u32[]{:S(2)}) %copy-start.6) | copy-done | bytes 12312
  8.8 0.0 copy-start.7
  8.8 0.7 %copy-done.7 = bf16[2048,2]{0,1:T(2,128)(2,1)S(1)} copy-done((bf16[2048,2]{0,1:T(2,128)(2,1)S(1)}, bf16[2048,2]{0,1:T(2,128)(2,1)}, u32[]{:S(2)}) %copy-start.7) | copy-done | bytes 8216
  9.5 0.0 copy-start.8
  9.5 0.7 %copy-done.8 = s32[12]{0:T(128)S(1)} copy-done((s32[12]{0:T(128)S(1)}, s32[12]{0:T(128)}, u32[]{:S(2)}) %copy-start.8) | copy-done | bytes 72
  10.1 0.0 copy-start.9
  10.1 0.7 %copy-done.9 = bf16[64]{0:T(256)(128)(2,1)S(1)} copy-done((bf16[64]{0:T(256)(128)(2,1)S(1)}, bf16[64]{0:T(256)(128)(2,1)}, u32[]{:S(2)}) %copy-start.9) | copy-done | bytes 152
  10.8 0.0 copy-start.10
  10.8 0.7 %copy-done.10 = bf16[64]{0:T(256)(128)(2,1)S(1)} copy-done((bf16[64]{0:T(256)(128)(2,1)S(1)}, bf16[64]{0:T(256)(128)(2,1)}, u32[]{:S(2)}) %copy-start.10) | copy-done | bytes 152
  11.4 21.8 %decode.1 = (bf16[12,512]{1,0:T(8,128)(2,1)S(1)}, bf16[12,1,64]{2,1,0:T(2,128)(2,1)S(1)}, bf16[12,1,64]{2,1,0:T(2,128)(2,1)S(1)}, f32[12,1]{1,0:T(8,128)S(1)}) custom-call(s32[12]{0:T(128)S(1)} %copy-done.8, bf16[12,512]{1,0:T(8,128)(2,1)S(1)} %copy-done.6, bf16[1,512]{1,0:T(2,128)(2,1)S(1)} %reshape.17.norm_gain_ref, bf16[1,64]{1,0:T(2,128)(2,1)S(1)} %bitcast.4, ...), custom_call_target="tpu_custom_call" | custom-call | tf_op jit(solution)/shard_map/decode/pallas_call | solution.py:383
  33.3 0.6 %copy.19 = f32[12,1]{0,1:T(1,128)} copy(f32[12,1]{1,0:T(8,128)S(1)} %get-tuple-element.7) | data formatting | bytes 96 | tf_op jit(solution)/shard_map/decode/pallas_call | solution.py:383
  33.9 0.6 %copy.17 = bf16[12,1,64]{2,0,1:T(8,128)(2,1)} copy(bf16[12,1,64]{2,1,0:T(2,128)(2,1)S(1)} %get-tuple-element.5) | data formatting | bytes 3072 | tf_op jit(solution)/shard_map/decode/pallas_call | solution.py:383
  34.5 0.6 %copy.18 = bf16[12,1,64]{2,0,1:T(8,128)(2,1)} copy(bf16[12,1,64]{2,1,0:T(2,128)(2,1)S(1)} %get-tuple-element.6) | data formatting | bytes 3072 | tf_op jit(solution)/shard_map/decode/pallas_call | solution.py:383
  35.1 0.6 %copy.21 = bf16[12,512]{1,0:T(8,128)(2,1)} copy(bf16[12,512]{1,0:T(8,128)(2,1)S(1)} %get-tuple-element.12) | data formatting | bytes 24576
Async XLA Ops:
  1.3 1.4 %copy-start = (bf16[12,1,64,1024]{3,2,1,0:T(8,128)(2,1)S(1)}, bf16[12,1,64,1024]{3,2,1,0:T(8,128)(2,1)}, u32[]{:S(2)}) copy-start(bf16[12,1,64,1024]{3,2,1,0:T(8,128)(2,1)} %key_hbm.1) | copy-start | bytes 4718596
  2.7 1.2 %copy-start.1 = (bf16[512,1024]{1,0:T(8,128)(2,1)S(1)}, bf16[512,1024]{1,0:T(8,128)(2,1)}, u32[]{:S(2)}) copy-start(bf16[512,1024]{1,0:T(8,128)(2,1)} %query_hbm.1) | copy-start | bytes 3145732
  3.9 1.2 %copy-start.2 = (bf16[1024,512]{1,0:T(8,128)(2,1)S(1)}, bf16[1024,512]{1,0:T(8,128)(2,1)}, u32[]{:S(2)}) copy-start(bf16[1024,512]{1,0:T(8,128)(2,1)} %output_hbm.1) | copy-start | bytes 3145732
  5.2 1.0 %copy-start.3 = (bf16[2048,128]{1,0:T(8,128)(2,1)S(1)}, bf16[2048,128]{1,0:T(8,128)(2,1)}, u32[]{:S(2)}) copy-start(bf16[2048,128]{1,0:T(8,128)(2,1)} %key_w_hbm.1) | copy-start | bytes 1572868
  6.2 1.0 %copy-start.4 = (bf16[2048,128]{1,0:T(8,128)(2,1)S(1)}, bf16[2048,128]{1,0:T(8,128)(2,1)}, u32[]{:S(2)}) copy-start(bf16[2048,128]{1,0:T(8,128)(2,1)} %value_w_hbm.1) | copy-start | bytes 1572868
  7.3 0.8 %copy-start.5 = (f32[12,1,1024]{2,1,0:T(1,128)S(1)}, f32[12,1,1024]{2,1,0:T(1,128)}, u32[]{:S(2)}) copy-start(f32[12,1,1024]{2,1,0:T(1,128)} %decay_hbm.1) | copy-start | bytes 147460
  8.1 0.7 %copy-start.6 = (bf16[12,512]{1,0:T(8,128)(2,1)S(1)}, bf16[12,512]{1,0:T(8,128)(2,1)}, u32[]{:S(2)}) copy-start(bf16[12,512]{1,0:T(8,128)(2,1)} %tokens_ref.1) | copy-start | bytes 36868
  8.8 0.7 %copy-start.7 = (bf16[2048,2]{0,1:T(2,128)(2,1)S(1)}, bf16[2048,2]{0,1:T(2,128)(2,1)}, u32[]{:S(2)}) copy-start(bf16[2048,2]{0,1:T(2,128)(2,1)} %param.18) | copy-start | bytes 24580
  9.5 0.7 %copy-start.8 = (s32[12]{0:T(128)S(1)}, s32[12]{0:T(128)}, u32[]{:S(2)}) copy-start(s32[12]{0:T(128)} %lengths_ref.1) | copy-start | bytes 148
  10.1 0.7 %copy-start.9 = (bf16[64]{0:T(256)(128)(2,1)S(1)}, bf16[64]{0:T(256)(128)(2,1)}, u32[]{:S(2)}) copy-start(bf16[64]{0:T(256)(128)(2,1)} %param.20) | copy-start | bytes 388
  10.8 0.7 %copy-start.10 = (bf16[64]{0:T(256)(128)(2,1)S(1)}, bf16[64]{0:T(256)(128)(2,1)}, u32[]{:S(2)}) copy-start(bf16[64]{0:T(256)(128)(2,1)} %param.21) | copy-start | bytes 388

commit v2 on v1

--- a/solution.py
+++ b/solution.py
@@ -50,6 +50,8 @@
     out_slots,
     query_rows,
     att_rows,
+    score_rows,
+    weight_rows,
     local_sem,
     query_send,
     query_recv,
@@ -141,7 +143,7 @@
             ).wait_recv()
 
     tokens = tokens_ref[...].astype(F32)
-    scaled = (tokens * norm_gain_ref[...].astype(F32)).astype(BF16)
+    scaled = (tokens * norm_gain_ref[...].astype(F32).reshape(1, width)).astype(BF16)
     for c in range(query_chunks):
         query_copies[c].wait()
         part = jnp.dot(scaled, query_w[c], preferred_element_type=F32)
@@ -185,8 +187,16 @@
     for copy in small_sends:
         copy.start()
 
+    scale = head_dim ** (-0.5)
+    decay_copy.wait()
+    positions = me * span + lax.broadcasted_iota(jnp.int32, (1, span), 1)
+    for b in range(rows):
+        decay[b] = jnp.where(positions < lengths_ref[b], decay[b], FLOOR)
+    key_copy.wait()
+    value_copy.wait()
+
     wait_recv(query_slots, query_send, query_recv)
-    gain = query_gain_ref[...].astype(F32)
+    gain = query_gain_ref[...].astype(F32).reshape(1, head_dim)
     gain2 = jnp.concatenate([gain, gain], axis=1)
 
     def norm_pair(x, gain_wide):
@@ -202,44 +212,51 @@
         x = query_slots[0, :, cols].astype(F32)
         for p in range(1, kv_n):
             x = x + query_slots[p, :, cols].astype(F32)
-        y = norm_pair(x, gain2)
+        y = norm_pair(x, gain2) * scale
         query_rows[pl.ds(2 * c, rows, stride=group), :] = y
         query_rows[pl.ds(2 * c + 1, rows, stride=group), :] = pltpu.roll(y, head_dim, 1)
 
-    key_copy.wait()
-    decay_copy.wait()
-    value_copy.wait()
-    scale = head_dim ** (-0.5)
-    positions = me * span + lax.broadcasted_iota(jnp.int32, (group, span), 1)
     lane = lax.broadcasted_iota(jnp.int32, (group, 128), 1)
     stat_max = jnp.full((group, 128), FLOOR, F32)
     stat_sum = jnp.zeros((group, 128), F32)
 
-    def attend(b, stat_max, stat_sum):
-        q = query_rows[group * b : group * (b + 1), 0:head_dim].astype(BF16)
-        scores = jnp.dot(q, keys[b], preferred_element_type=F32) * scale + decay[b]
-        valid = positions < lengths_ref[b]
-        block_max = jnp.max(jnp.where(valid, scores, FLOOR), axis=1, keepdims=True)
-        weights = jnp.where(valid, jnp.exp(scores - block_max), 0.0)
-        block_sum = jnp.sum(weights, axis=1, keepdims=True)
-        result = lax.dot_general(
-            weights.astype(BF16), values[b], (((1,), (1,)), ((), ())), preferred_element_type=F32
-        )
-        stat_max = jnp.where(lane == b, block_max, stat_max)
-        stat_sum = jnp.where(lane == b + 32, block_sum, stat_sum)
-        return result, stat_max, stat_sum
+    def rows_of(b):
+        return slice(group * b, group * (b + 1))
 
     value_sends = []
-    for i in range(pairs):
-        one, stat_max, stat_sum = attend(i, stat_max, stat_sum)
-        two, stat_max, stat_sum = attend(i + pairs, stat_max, stat_sum)
-        value_slots[me, i] = jnp.concatenate([one, two], axis=1).astype(BF16)
-        if (i + 1) % per_chunk == 0:
-            index = pl.ds(i + 1 - per_chunk, per_chunk)
-            new = sends(value_slots, value_send, value_recv, index)
-            for copy in new:
-                copy.start()
-            value_sends += new
+    for chunk in range(chunks):
+        first_pair = chunk * per_chunk
+        members = []
+        for i in range(first_pair, first_pair + per_chunk):
+            members += [i, i + pairs]
+        maxes = {}
+        for b in members:
+            q = query_rows[rows_of(b), 0:head_dim].astype(BF16)
+            scores = jnp.dot(q, keys[b], preferred_element_type=F32) + decay[b]
+            score_rows[rows_of(b), :] = scores
+            maxes[b] = jnp.max(scores, axis=1, keepdims=True)
+            stat_max = jnp.where(lane == b, maxes[b], stat_max)
+        for b in members:
+            weights = jnp.exp(score_rows[rows_of(b), :] - maxes[b])
+            weight_rows[rows_of(b), :] = weights.astype(BF16)
+            block_sum = jnp.sum(weights, axis=1, keepdims=True)
+            stat_sum = jnp.where(lane == b + 32, block_sum, stat_sum)
+        results = {}
+        for b in members:
+            results[b] = lax.dot_general(
+                weight_rows[rows_of(b), :],
+                values[b],
+                (((1,), (1,)), ((), ())),
+                preferred_element_type=F32,
+            )
+        for i in range(first_pair, first_pair + per_chunk):
+            value_slots[me, i] = jnp.concatenate(
+                [results[i], results[i + pairs]], axis=1
+            ).astype(BF16)
+        new = sends(value_slots, value_send, value_recv, pl.ds(first_pair, per_chunk))
+        for copy in new:
+            copy.start()
+        value_sends += new
     half = group // 2
     packed = jnp.where(lane < 32, stat_max, stat_sum)
     stat_slots[me] = jnp.where(
@@ -256,20 +273,21 @@
     row_scale_row = lax.rsqrt(small[rows + 1 : rows + 2] / model + EPSILON)
     gate_x = row_scale_row * small[rows : rows + 1]
     gate = jnp.minimum(gate_x, 0.0) - jnp.log1p(jnp.exp(-jnp.abs(gate_x)))
-    new_gate_ref[...] = to_column(gate)
-    key_gain = key_gain_ref[...].astype(F32)
+    new_gate_ref[...] = gate[:, 0:rows]
+    key_gain = key_gain_ref[...].astype(F32).reshape(1, head_dim)
     both = small[:rows]
     new_key = norm_pair(both, jnp.concatenate([key_gain, key_gain], axis=1))
     new_value = (both * to_column(row_scale_row)).astype(BF16).astype(F32)
+    new_value_turned = pltpu.roll(new_value, head_dim, 1)
+    new_key_ref[...] = new_key[:, 0:head_dim].astype(BF16)
+    new_value_ref[...] = new_value_turned[:, 0:head_dim].astype(BF16)
     own = jnp.zeros((group, 128), F32)
     for b in range(rows):
-        new_key_ref[b] = new_key[b : b + 1, 0:head_dim].astype(BF16)
-        new_value_ref[b] = new_value[b : b + 1, head_dim:].astype(BF16)
         q = query_rows[group * b : group * (b + 1), :]
         dots = jnp.sum(
             jnp.where(lane < head_dim, q * new_key[b : b + 1], 0.0), axis=1, keepdims=True
         )
-        own = jnp.where(lane == b, dots * scale, own)
+        own = jnp.where(lane == b, dots, own)
 
     wait_recv(stat_slots, stat_send, stat_recv)
     maxima, totals = [], []
@@ -294,7 +312,6 @@
     def spread(f, i):
         return jnp.where(lane < head_dim, f[:, i : i + 1], f[:, i + pairs : i + pairs + 1])
 
-    new_value_turned = pltpu.roll(new_value, head_dim, 1)
     for c in range(chunks):
         wait_recv(value_slots, value_send, value_recv, pl.ds(c * per_chunk, per_chunk))
         for i in range(c * per_chunk, (c + 1) * per_chunk):
@@ -351,6 +368,12 @@
         copy.wait_send()
 
 
+def emit(*refs):
+    half = len(refs) // 2
+    for source, target in zip(refs[:half], refs[half:]):
+        target[...] = source[...]
+
+
 def on_device(
     kv_n,
     tp_n,
@@ -378,15 +401,15 @@
     pairs = rows // 2
     small_rows = -(-(rows + 2) // 8) * 8
     vmem = pl.BlockSpec(memory_space=pltpu.VMEM)
-    hbm = pl.BlockSpec(memory_space=pl.ANY)
+    hbm = pl.BlockSpec(memory_space=pltpu.HBM)
     dma = pltpu.SemaphoreType.DMA
-    return pl.pallas_call(
+    results = pl.pallas_call(
         functools.partial(kernel, kv_n, tp_n),
         out_shape=(
             jax.ShapeDtypeStruct((rows, out_cols), BF16),
-            jax.ShapeDtypeStruct((rows, 1, head_dim), BF16),
-            jax.ShapeDtypeStruct((rows, 1, head_dim), BF16),
-            jax.ShapeDtypeStruct((rows, 1), F32),
+            jax.ShapeDtypeStruct((rows, head_dim), BF16),
+            jax.ShapeDtypeStruct((rows, head_dim), BF16),
+            jax.ShapeDtypeStruct((1, rows), F32),
         ),
         in_specs=[pl.BlockSpec(memory_space=pltpu.SMEM)] + [vmem] * 4 + [hbm] * 8,
         out_specs=(vmem, vmem, vmem, vmem),
@@ -406,6 +429,8 @@
             pltpu.VMEM((tp_n, rows, out_cols), BF16),
             pltpu.VMEM((rows * heads, 128), F32),
             pltpu.VMEM((rows, heads * head_dim), F32),
+            pltpu.VMEM((rows * heads, span), F32),
+            pltpu.VMEM((rows * heads, span), BF16),
             dma((query_chunks + 7,)),
             dma((kv_n,)),
             dma((kv_n,)),
@@ -419,15 +444,15 @@
             dma((tp_n,)),
         ],
         compiler_params=pltpu.CompilerParams(
-            collective_id=0, has_side_effects=True, vmem_limit_bytes=48 * 1024 * 1024
+            collective_id=0, has_side_effects=True, vmem_limit_bytes=67043328
         ),
         name="decode",
     )(
         lengths,
         tokens,
-        norm_gain.reshape(1, width),
-        query_gain.reshape(1, head_dim),
-        key_gain.reshape(1, head_dim),
+        norm_gain,
+        query_gain,
+        key_gain,
         gate_weight.T,
         query_weight,
         key_weight,
@@ -436,6 +461,20 @@
         key_cache,
         value_cache,
         decay_cache,
+    )
+    mixed, new_key, new_value, new_gate = pl.pallas_call(
+        emit,
+        out_shape=tuple(jax.ShapeDtypeStruct(r.shape, r.dtype) for r in results),
+        in_specs=[vmem] * 4,
+        out_specs=(vmem,) * 4,
+        compiler_params=pltpu.CompilerParams(vmem_limit_bytes=67043328),
+        name="emit",
+    )(*results)
+    return (
+        mixed,
+        new_key.reshape(rows, 1, head_dim),
+        new_value.reshape(rows, 1, head_dim),
+        new_gate.T,
     )
 
 

time: 36.2 us -> 24.4 us (0.67)
  local copies, waits for them, and re-layouts: 13.2 us -> 0 us
  Pallas kernels: 21.8 us -> 23.5 us
    unnamed x23 -> x0, local copies, waits for them, and re-layouts: 10.7 us -> none
    pallas_call x3 -> x0, local copies, waits for them, and re-layouts: 1.78 us -> none  [on_device(): pl.pallas_call(functools.partial(kernel, kv_n, tp_n), out_shape=(jax.Shap...]
    pallas_call x0 -> x1, Pallas kernels: none -> 1.34 us  [on_device(): pl.pallas_call(emit, out_shape=tuple((jax.ShapeDtypeStruct(r.shape, r.dty...]
    reshape x1 -> x0, local copies, waits for them, and re-layouts: 0.68 us -> none  [on_device(): norm_gain.reshape(1, width)]
where the time goes in v2:
time: 24.4 us; the launch traced here: 24.2 us
  Pallas kernels  23.5 us (96%)
  between operations  0.64 us (3%)
    pallas_call x1, Pallas kernels, on_device(): pl.pallas_call(functools.partial(kernel, kv_n, tp_n), out_shape=(jax.Shap...  22.2 us
    pallas_call x1, Pallas kernels, on_device(): pl.pallas_call(emit, out_shape=tuple((jax.ShapeDtypeStruct(r.shape, r.dty...  1.34 us

profile of v2, /device:TPU:0, one launch (start us, length us, event | category | flops | bytes accessed | tf_op | source)
XLA Modules:
  0.0 24.2 jit_solution(11582074782215794147)
XLA Ops:
  0.6 22.2 %decode.1 = (bf16[12,512]{1,0:T(8,128)(2,1)}, bf16[12,64]{1,0:T(8,128)(2,1)}, bf16[12,64]{1,0:T(8,128)(2,1)}, f32[1,12]{1,0:T(1,128)}) custom-call(s32[12]{0:T(128)} %lengths_ref.1, bf16[12,512]{1,0:T(8,128)(2,1)} %tokens_ref.1, bf16[512]{0:T(512)(128)(2,1)} %norm_gain_ref.1, bf16[64]{0:T(256)(128)(2,1)} %query_gain_ref.1, bf16[64]{0:T(256)(128)(2,1)} %key_gain_ref.1, ...), custom_call_target="tpu_custom_call" | custom-call | tf_op jit(solution)/shard_map/decode/pallas_call | solution.py:406
  22.8 1.3 %emit.1 = (bf16[12,512]{1,0:T(8,128)(2,1)}, bf16[12,64]{1,0:T(8,128)(2,1)}, bf16[12,64]{1,0:T(8,128)(2,1)}, f32[1,12]{1,0:T(1,128)}) custom-call(bf16[12,512]{1,0:T(8,128)(2,1)} %get-tuple-element.12.refs_0_, bf16[12,64]{1,0:T(8,128)(2,1)} %get-tuple-element.13.refs_1_, bf16[12,64]{1,0:T(8,128)(2,1)} %get-tuple-element.14.refs_2_, ...), custom_call_target="tpu_custom_call" | custom-call | tf_op jit(solution)/shard_map/emit/pallas_call | solution.py:465
